TPU v7x, 256 devices: a whole 4x4x8 slice. The times are simulated.
256 devices in a mesh: sp: 64 (over z, y, core), tp: 4 (over x).
Axes of the slice: x: 4, y: 4, z: 8, core: 2. Of those that a mesh axis runs over, the one named last changes fastest.
Arguments:
- resid: bfloat16 [24576, 2048], P(('sp', 'tp')), may hold values from -6 to 6
- conv_b: bfloat16 [24576, 1024], P('sp', 'tp'), may hold values from -6 to 6
- conv_c: bfloat16 [24576, 1024], P('sp', 'tp'), may hold values from -6 to 6
- conv_x: bfloat16 [24576, 1024], P('sp', 'tp'), may hold values from -6 to 6
- conv_taps: bfloat16 [3, 1024], P(None, 'tp'), may hold values from -3.5 to 3.5
- out_weight: bfloat16 [1024, 2048], P('tp'), may hold values from -0.1875 to 0.1875
- norm_gain: float32 [2048], replicated, may hold values from 0.1 to 1.9
- routes: int32 [24576, 2], P('sp'), may hold values from 0 to 63, all different within a row; in each aligned block of 96 rows (0 to 95, 96 to 191, ...) at most 4 rows name the same one
- route_weight: float32 [24576, 2], P('sp'), may hold values from 0.2 to 1
- expert_gate: bfloat16 [64, 2048, 1024], P('sp', None, 'tp'), may hold values from -0.125 to 0.125
- expert_up: bfloat16 [64, 2048, 1024], P('sp', None, 'tp'), may hold values from -0.125 to 0.125
- expert_down: bfloat16 [64, 1024, 2048], P('sp', 'tp'), may hold values from -0.1875 to 0.1875
- shared_gate: bfloat16 [2048, 1024], P(None, 'tp'), may hold values from -0.125 to 0.125
- shared_up: bfloat16 [2048, 1024], P(None, 'tp'), may hold values from -0.125 to 0.125
- shared_down: bfloat16 [1024, 2048], P('tp'), may hold values from -0.1875 to 0.1875
Outputs:
- layer_out: bfloat16 [24576, 2048], P(('sp', 'tp'))
Inputs may be any that keep to these rules, and one draw needn't show every extreme that they name: `routes`: in each aligned block of 96 tokens no expert is named more than 4 times; in some blocks some expert is named exactly 4 times; each row names 2 different experts.
All inputs are finite; a program needn't handle non-finite values.
Results may differ from a plain program's by a relative error of at most 0.015.
Values may be sent and summed in bfloat16 or wider, within the bound.
A program may use at most 128 MiB of HBM per device.

v0:
```python
import jax
import jax.numpy as jnp
from jax import lax
from jax.sharding import PartitionSpec as P


def shifted(block, axis, distance):
    devices = range(lax.axis_size(axis))
    route = [(i - distance, i) for i in devices if i - distance in devices]
    return lax.ppermute(block, axis, route)


def round_trip(values):
    return lax.optimization_barrier(values.astype(jnp.bfloat16)).astype(jnp.float32)


def rank_slots(route_rows, expert_count, tp_parts):
    flat_routes = route_rows.reshape(tp_parts, -1)
    onehot = (
        flat_routes[:, :, None] == jnp.arange(expert_count, dtype=jnp.int32)[None, None, :]
    ).astype(jnp.int32)
    slot_ranks = jnp.sum((jnp.cumsum(onehot, axis=1) - 1) * onehot, axis=2)
    return (flat_routes, slot_ranks)


def local(
    resid,
    conv_b,
    conv_c,
    conv_x,
    conv_taps,
    out_weight,
    norm_gain,
    routes,
    route_weight,
    expert_gate,
    expert_up,
    expert_down,
    shared_gate,
    shared_up,
    shared_down,
):
    tok_dev = conv_b.shape[0]
    tp_parts = lax.axis_size("tp")
    groups = lax.axis_size("sp")
    quarter = tok_dev // tp_parts
    tap_count = conv_taps.shape[0]
    exp_dev = expert_gate.shape[0]
    expert_count = exp_dev * groups
    model_width = resid.shape[1]
    top_count = routes.shape[1]
    capacity = max(2, 3 * quarter * top_count // (2 * expert_count))
    my_part = lax.axis_index("tp")
    product = conv_c.astype(jnp.float32) * conv_x.astype(jnp.float32)
    rim_rows = shifted(product[tok_dev - (tap_count - 1) :], "sp", 1)
    padded = jnp.concatenate([rim_rows, product], 0)
    conv_sum = padded[0:tok_dev] * conv_taps[0].astype(jnp.float32)
    for tap_index in range(1, tap_count):
        conv_sum = conv_sum + padded[tap_index : tap_index + tok_dev] * conv_taps[tap_index].astype(
            jnp.float32
        )
    mixed_rows = (conv_b.astype(jnp.float32) * conv_sum).astype(jnp.bfloat16)
    projected = lax.psum_scatter(
        round_trip(jnp.dot(mixed_rows, out_weight, preferred_element_type=jnp.float32)).astype(
            jnp.bfloat16
        ),
        "tp",
        scatter_dimension=0,
        tiled=True,
    ).astype(jnp.float32)
    middle = (resid.astype(jnp.float32) + projected).astype(jnp.bfloat16)
    middle_float = middle.astype(jnp.float32)
    inv_scale = lax.rsqrt(jnp.mean(middle_float * middle_float, axis=-1, keepdims=True) + 1e-06)
    normed = (middle_float * inv_scale * norm_gain).astype(jnp.bfloat16)
    flat_routes, slot_ranks = rank_slots(routes, expert_count, tp_parts)
    own_routes = lax.dynamic_index_in_dim(flat_routes, my_part, 0, keepdims=False)
    own_ranks = lax.dynamic_index_in_dim(slot_ranks, my_part, 0, keepdims=False)
    slot_ids = own_routes * capacity + own_ranks
    token_ids = jnp.repeat(jnp.arange(quarter, dtype=jnp.int32), top_count)
    slot_token = (
        jnp.full((expert_count * capacity,), quarter, jnp.int32).at[slot_ids].set(token_ids)
    )
    padded_rows = jnp.concatenate([normed, jnp.zeros((1, model_width), jnp.bfloat16)], 0)
    outgoing = padded_rows[slot_token].reshape(groups, exp_dev * capacity, model_width)
    arrived = lax.all_to_all(outgoing, "sp", split_axis=0, concat_axis=0, tiled=True)
    arrived = arrived.reshape(groups, exp_dev, capacity, model_width)
    arrived, group_normed = (
        lax.all_gather(arrived, "tp", axis=2, tiled=True),
        lax.all_gather(normed, "tp", axis=0, tiled=True),
    )
    gate_val = jnp.einsum(
        "gerd,edf->gerf", arrived, expert_gate, preferred_element_type=jnp.float32
    )
    up_val = jnp.einsum("gerd,edf->gerf", arrived, expert_up, preferred_element_type=jnp.float32)
    hidden = (jax.nn.silu(gate_val) * up_val).astype(jnp.bfloat16)
    partial_rows = round_trip(
        jnp.einsum("gerf,efd->gerd", hidden, expert_down, preferred_element_type=jnp.float32)
    )
    shared_gate_val = jnp.dot(group_normed, shared_gate, preferred_element_type=jnp.float32)
    shared_up_val = jnp.dot(group_normed, shared_up, preferred_element_type=jnp.float32)
    shared_hidden = (jax.nn.silu(shared_gate_val) * shared_up_val).astype(jnp.bfloat16)
    shared_part = round_trip(
        jnp.dot(shared_hidden, shared_down, preferred_element_type=jnp.float32)
    )
    summed, shared = (
        lax.psum_scatter(
            partial_rows.astype(jnp.bfloat16), "tp", scatter_dimension=2, tiled=True
        ).astype(jnp.float32),
        lax.psum_scatter(
            shared_part.astype(jnp.bfloat16), "tp", scatter_dimension=0, tiled=True
        ).astype(jnp.float32),
    )
    returned = lax.all_to_all(
        summed.astype(jnp.bfloat16), "sp", split_axis=0, concat_axis=0, tiled=True
    )
    returned = returned.reshape(expert_count * capacity, model_width)
    picked = returned[own_routes * capacity + own_ranks].reshape(quarter, top_count, model_width)
    own_weights = lax.dynamic_slice_in_dim(route_weight, my_part * quarter, quarter, 0)
    routed = jnp.sum(picked.astype(jnp.float32) * own_weights[:, :, None], axis=1)
    return (middle.astype(jnp.float32) + shared + routed).astype(jnp.bfloat16)


def solution(mesh):
    return jax.shard_map(
        local,
        mesh=mesh,
        in_specs=(
            P(("sp", "tp"), None),
            P("sp", "tp"),
            P("sp", "tp"),
            P("sp", "tp"),
            P(None, "tp"),
            P("tp", None),
            P(),
            P("sp", None),
            P("sp", None),
            P("sp", None, "tp"),
            P("sp", None, "tp"),
            P("sp", "tp", None),
            P(None, "tp"),
            P(None, "tp"),
            P("tp", None),
        ),
        out_specs=P(("sp", "tp"), None),
        check_vma=False,
    )
```

profile of v0, /device:TPU:1, one launch (start us, length us, event | category | flops | bytes accessed | tf_op | source)
XLA Modules:
  0.0 281.4 jit_solution(15139405090504358709)
XLA Ops:
  6.5 0.0 copy-start
  6.5 0.0 reduce-scatter.4.cloned.1.call-start
  6.5 1.1 convert_multiply_fusion.2
  7.7 4.6 %collective-permute-start = (f32[2,256]{1,0:T(2,128)S(1)}, f32[2,256]{1,0:T(2,128)S(1)}, u32[]{:S(2)}, u32[]{:S(2)}) collective-permute-start(f32[2,256]{1,0:T(2,128)S(1)} %slice.40), channel_id=1, source_target_pairs={{0,4},{4,8},{8,12},{12,16},{16,20},{20,24},{24,28},{28,32},{32,36}... | collective-permute-start | bytes 6152 | tf_op jit(solution)/shard_map/ppermute | solution.py:10
  12.3 0.8 slice_convert_fusion.2
  13.1 0.0 collective-permute-done
  13.1 3.2 %convolution_convert_fusion.1 = bf16[384,2048]{1,0:T(8,128)(2,1)} fusion(bf16[256,2048]{1,0:T(8,128)(2,1)} %param.20, f32[2,256]{1,0:T(2,128)S(1)} %collective-permute-done, f32[384,256]{1,0:T(8,128)S(1)} %convert_multiply_fusion.2, bf16[384,256]{1,0:T(8,128)(2,1)} %param.16, f32[256]{0:T(256)S(1)} %bitcast.68, f32[256]{0:T(256)S(1)} %bitcast.69, ...), kind=kOutput, calls=%fused_computation.5 | convolution fusion | flops 404422656 | bytes 3216384 | tf_op jit(solution)/shard_map/dot_general | solution.py:64
  16.3 0.0 reduce-scatter.4.cloned.1.call-update
  16.3 0.0 copy-start.1
  16.3 0.0 all-gather.6.cloned.1.call-start
  16.3 0.6 copy-done.6
  16.9 0.1 copy.34
  17.1 0.2 reshape.92
  17.3 0.0 copy-start.5
  17.3 2.4 reduce-window.6
  19.7 0.1 slice.43
  19.9 0.1 copy.36
  20.0 0.1 reshape.129
  20.2 0.1 bitcast_bitcast_fusion
  20.3 0.1 fusion.26
  20.4 1.2 scatter_custom_fusion
  21.6 26.1 %reduce-scatter.4.cloned.1.call-done = bf16[96,2048]{1,0:T(8,128)(2,1)} async-done(((bf16[384,2048]{1,0:T(8,128)(2,1)}), bf16[96,2048]{1,0:T(8,128)(2,1)}) %reduce-scatter.4.cloned.1.call-update) | async-done | bytes 393232 | tf_op jit(solution)/shard_map/reduce_scatter | solution.py:63
  47.8 0.0 copy-done.1
  47.8 1.2 fusion.7
  49.0 0.0 copy-done.5
  49.0 1.2 fusion.9
  50.2 0.0 copy-start.3
  50.2 0.7 copy-done.3
  50.9 1.4 gather_fusion
  52.3 0.4 reshape.96
  52.8 39.5 %all_to_all.10 = bf16[64,4,2048]{2,1,0:T(4,128)(2,1)S(1)} all-to-all(bf16[64,4,2048]{2,1,0:T(4,128)(2,1)S(1)} %reshape.96), channel_id=1, replica_groups=mesh['sp'=64,'tp'=4] {'sp'}, dimensions={0} | all-to-all | bytes 2097152 | tf_op jit(solution)/shard_map/all_to_all | solution.py:85
  92.2 1.6 copy.39
  93.8 0.0 all-gather.6.cloned.1.call-update
  93.9 0.0 all-gather.4.cloned.1.call-start
  93.9 0.7 all-gather.4.cloned.1.call-update
  94.6 0.0 copy-start.10
  94.6 0.0 reduce-scatter.8.cloned.1.call-start
  94.7 45.3 %all-gather.6.cloned.1.call-done = bf16[64,16,2048]{2,0,1:T(8,128)(2,1)} async-done(((bf16[64,4,2048]{2,0,1:T(8,128)(2,1)}), bf16[64,16,2048]{2,0,1:T(8,128)(2,1)}) %all-gather.6.cloned.1.call-update) | async-done | bytes 4194320 | tf_op jit(solution)/shard_map/all_gather | solution.py:88
  140.0 0.0 copy-done.9
  140.0 3.6 %convolution_bitcast_fusion.1 = f32[64,1,16,256]{3,0,2,1:T(8,128)S(1)} fusion(bf16[64,16,2048]{2,0,1:T(8,128)(2,1)} %all-gather.6.cloned.1.call-done, bf16[1,2048,256]{2,1,0:T(8,128)(2,1)S(1)} %copy-done.9), kind=kOutput, calls=%fused_computation.9 | convolution fusion | flops 1073741824 | bytes 6291456 | tf_op jit(solution)/shard_map/gerd,edf->gerf/dot_general | solution.py:91
  143.6 0.0 copy-done.10
  143.6 1.3 fusion.2
  144.9 1.4 convert_bitcast_fusion
  146.3 4.2 %copy.41 = bf16[64,1,16,2048]{3,0,1,2:T(8,128)(2,1)} copy(bf16[64,1,16,2048]{3,2,0,1:T(8,128)(2,1)S(1)} %convert_bitcast_fusion) | data formatting | bytes 8388608 | tf_op jit(solution)/shard_map/optimization_barrier | solution.py:14
  150.5 0.0 reduce-scatter.8.cloned.1.call-update
  150.6 0.2 reduce-scatter.6.cloned.1.call-start
  150.8 20.4 %all-gather.4.cloned.1.call-done = bf16[384,2048]{1,0:T(8,128)(2,1)} async-done(((bf16[96,2048]{1,0:T(8,128)(2,1)}), bf16[384,2048]{1,0:T(8,128)(2,1)}) %all-gather.4.cloned.1.call-update) | async-done | bytes 1572880 | tf_op jit(solution)/shard_map/all_gather | solution.py:89
  171.2 2.4 fusion.38
  173.6 0.0 copy-done.8
  173.6 4.5 %convolution_convert_fusion = bf16[384,2048]{1,0:T(8,128)(2,1)} fusion(bf16[256,2048]{1,0:T(8,128)(2,1)} %param.29, bf16[384,2048]{1,0:T(8,128)(2,1)S(1)} %copy-done.8, bf16[2048,256]{1,0:T(8,128)(2,1)} %param.28, f32[384,256]{1,0:T(8,128)S(1)} %fusion.38), kind=kOutput, calls=%fused_computation.4 | convolution fusion | flops 806682624 | bytes 5636096 | tf_op jit(solution)/shard_map/dot_general | solution.py:103
  178.1 0.0 reduce-scatter.6.cloned.1.call-update
  178.2 44.9 %reduce-scatter.8.cloned.1.call-done = bf16[64,1,4,2048]{3,0,1,2:T(8,128)(2,1)} async-done(((bf16[64,1,16,2048]{3,0,1,2:T(8,128)(2,1)}), bf16[64,1,4,2048]{3,0,1,2:T(8,128)(2,1)}) %reduce-scatter.8.cloned.1.call-update) | async-done | bytes 1048592 | tf_op jit(solution)/shard_map/reduce_scatter | solution.py:106
  223.1 3.0 %copy.42 = bf16[64,1,4,2048]{3,2,1,0:T(4,128)(2,1)} copy(bf16[64,1,4,2048]{3,0,1,2:T(8,128)(2,1)} %reduce-scatter.8.cloned.1.call-done) | data formatting | bytes 2097152 | tf_op jit(solution)/shard_map/reduce_scatter | solution.py:106
  226.1 10.8 %all-to-all-start.1 = ((bf16[64,1,4,2048]{3,2,1,0:T(4,128)(2,1)}), bf16[64,1,4,2048]{3,2,1,0:T(4,128)(2,1)S(1)}, u32[]{:S(2)}, u32[]{:S(2)}) async-start(bf16[64,1,4,2048]{3,2,1,0:T(4,128)(2,1)} %copy.42), calls=%async_computation.4 | async-start | bytes 2097152 | tf_op jit(solution)/shard_map/all_to_all | solution.py:113
  236.9 0.8 constant_dynamic-slice_fusion
  237.7 0.7 copy.43
  238.4 26.7 %all-to-all-done.1 = bf16[64,1,4,2048]{3,2,1,0:T(4,128)(2,1)S(1)} async-done(((bf16[64,1,4,2048]{3,2,1,0:T(4,128)(2,1)}), bf16[64,1,4,2048]{3,2,1,0:T(4,128)(2,1)S(1)}, u32[]{:S(2)}, u32[]{:S(2)}) %all-to-all-start.1) | async-done | bytes 1048608 | tf_op jit(solution)/shard_map/all_to_all | solution.py:113
  265.1 0.3 reshape.103
  265.3 2.0 gather_fusion.1
  267.4 2.2 reshape.108
  269.5 0.0 copy-done.4
  269.5 0.0 copy-start.2
  269.6 3.2 %multiply_reduce_fusion = f32[96,2048]{1,0:T(8,128)} fusion(f32[96,2,2048]{2,1,0:T(2,128)S(1)} %reshape.108, f32[96,2]{1,0:T(8,128)S(1)} %copy-done.4), kind=kLoop, calls=%fused_computation.6 | loop fusion | flops 589824 | bytes 2360064 | tf_op jit(solution)/shard_map/reduce_sum | solution.py:119
  272.7 2.2 fusion.11
  (22 shorter events, 0.2 us)
Async XLA Ops:
  6.5 138.4 %copy-start = (bf16[1,256,2048]{2,1,0:T(8,128)(2,1)S(1)}, bf16[1,256,2048]{2,1,0:T(8,128)(2,1)}, u32[]{:S(2)}) copy-start(bf16[1,256,2048]{2,1,0:T(8,128)(2,1)} %param.26) | copy-start | bytes 3145732
  6.5 41.2 %reduce-scatter.4.cloned.1.call-start = ((), (), s32[]{:S(2)}) async-start(), calls=%async_computation.5 | async-start | bytes 1966080 | tf_op jit(solution)/shard_map/reduce_scatter | solution.py:63
  7.7 5.4 %collective-permute-start = (f32[2,256]{1,0:T(2,128)S(1)}, f32[2,256]{1,0:T(2,128)S(1)}, u32[]{:S(2)}, u32[]{:S(2)}) collective-permute-start(f32[2,256]{1,0:T(2,128)S(1)} %slice.40), channel_id=1, source_target_pairs={{0,4},{4,8},{8,12},{12,16},{16,20},{20,24},{24,28},{28,32},{32,36}... | collective-permute-start | bytes 6152 | tf_op jit(solution)/shard_map/ppermute | solution.py:10
  16.3 0.7 copy-start.6
  16.3 31.5 %copy-start.1 = (bf16[96,2048]{1,0:T(8,128)(2,1)S(1)}, bf16[96,2048]{1,0:T(8,128)(2,1)}, u32[]{:S(2)}) copy-start(bf16[96,2048]{1,0:T(8,128)(2,1)} %param.15) | copy-start | bytes 1179652
  16.3 123.7 %all-gather.6.cloned.1.call-start = ((), (), s32[]{:S(2)}) async-start(), calls=%async_computation.9 | async-start | bytes 5242880 | tf_op jit(solution)/shard_map/all_gather | solution.py:88
  17.3 31.7 %copy-start.5 = (f32[2048]{0:T(1024)S(1)}, f32[2048]{0:T(1024)}, u32[]{:S(2)}) copy-start(f32[2048]{0:T(1024)} %param.21) | copy-start | bytes 24580
  50.2 0.7 copy-start.3
  92.2 47.8 %copy-start.9 = (bf16[1,2048,256]{2,1,0:T(8,128)(2,1)S(1)}, bf16[1,2048,256]{2,1,0:T(8,128)(2,1)}, u32[]{:S(2)}) copy-start(bf16[1,2048,256]{2,1,0:T(8,128)(2,1)} %param.24) | copy-start | bytes 3145732
  93.9 77.3 %all-gather.4.cloned.1.call-start = ((), (), s32[]{:S(2)}) async-start(), calls=%async_computation.6 | async-start | bytes 1966080 | tf_op jit(solution)/shard_map/all_gather | solution.py:89
  94.6 49.0 %copy-start.10 = (bf16[1,2048,256]{2,1,0:T(8,128)(2,1)S(1)}, bf16[1,2048,256]{2,1,0:T(8,128)(2,1)}, u32[]{:S(2)}) copy-start(bf16[1,2048,256]{2,1,0:T(8,128)(2,1)} %param.25) | copy-start | bytes 3145732
  94.6 128.5 %reduce-scatter.8.cloned.1.call-start = ((), (), s32[]{:S(2)}) async-start(), calls=%async_computation.8 | async-start | bytes 5242880 | tf_op jit(solution)/shard_map/reduce_scatter | solution.py:106
  140.0 3.6 %copy-start.7 = (bf16[64,16,2048]{2,0,1:T(8,128)(2,1)S(1)}, bf16[64,16,2048]{2,0,1:T(8,128)(2,1)}, u32[]{:S(2)}) copy-start(bf16[64,16,2048]{2,0,1:T(8,128)(2,1)} %all-gather.6.cloned.1.call-done) | copy-start | bytes 12582916
  150.6 122.2 %reduce-scatter.6.cloned.1.call-start = ((), (), s32[]{:S(2)}) async-start(), calls=%async_computation.7 | async-start | bytes 1966080 | tf_op jit(solution)/shard_map/reduce_scatter | solution.py:109
  171.2 2.4 copy-start.8
  226.1 38.9 %all-to-all-start.1 = ((bf16[64,1,4,2048]{3,2,1,0:T(4,128)(2,1)}), bf16[64,1,4,2048]{3,2,1,0:T(4,128)(2,1)S(1)}, u32[]{:S(2)}, u32[]{:S(2)}) async-start(bf16[64,1,4,2048]{3,2,1,0:T(4,128)(2,1)} %copy.42), calls=%async_computation.4 | async-start | bytes 2097152 | tf_op jit(solution)/shard_map/all_to_all | solution.py:113
  267.4 2.2 copy-start.4
  269.5 3.2 %copy-start.2 = (bf16[96,2048]{1,0:T(8,128)(2,1)S(1)}, bf16[96,2048]{1,0:T(8,128)(2,1)}, u32[]{:S(2)}) copy-start(bf16[96,2048]{1,0:T(8,128)(2,1)} %reduce-scatter.4.cloned.1.call-done) | copy-start | bytes 1179652
Sparse Core Ops, SparseCore 0:
  16.4 31.3 reduce-scatter.3
  94.0 45.9 all-gather.5
  141.8 29.3 all-gather.3
  173.6 49.4 reduce-scatter.7
  225.5 27.2 reduce-scatter.5
where the time goes:
time: 282 us; the launch traced here: 281 us
  waiting for transfers between devices  164 us (58%)
  blocking collectives  39.5 us (14%)
  local copies, waits for them, and re-layouts  19.9 us (7%)
  matrix products  16.3 us (6%)
  starting transfers between devices  15.7 us (6%)
  between operations  13.4 us (5%)
  other arithmetic  12.4 us (4%)
    all_gather x1, waiting for transfers between devices, local(): lax.all_gather(arrived, 'tp', axis=2, tiled=True)  45.3 us
    reduce_scatter x1, waiting for transfers between devices, local(): lax.psum_scatter(partial_rows.astype(jnp.bfloat16), 'tp', scatter_dimensi...  44.9 us
    all_to_all x1, blocking collectives, local(): lax.all_to_all(outgoing, 'sp', split_axis=0, concat_axis=0, tiled=True)  39.5 us
    all_to_all x1, waiting for transfers between devices, local(): lax.all_to_all(summed.astype(jnp.bfloat16), 'sp', split_axis=0, concat_ax...  26.7 us
    reduce_scatter x1, waiting for transfers between devices, local(): lax.psum_scatter(round_trip(jnp.dot(mixed_rows, out_weight, preferred_ele...  26.1 us
    all_gather x1, waiting for transfers between devices, local(): lax.all_gather(normed, 'tp', axis=0, tiled=True)  20.4 us
    all_to_all x1, starting transfers between devices, local(): lax.all_to_all(summed.astype(jnp.bfloat16), 'sp', split_axis=0, concat_ax...  10.8 us
  transfers between devices with their start and end apart: 7, of which 5 were waited for; matrix products, arithmetic and copies ran while one was open for 12% of the time, Pallas kernels for 0%

commit v1 on v0

--- a/solution.py
+++ b/solution.py
@@ -86,7 +86,9 @@
     arrived = arrived.reshape(groups, exp_dev, capacity, model_width)
     arrived, group_normed = (
         lax.all_gather(arrived, "tp", axis=2, tiled=True),
-        lax.all_gather(normed, "tp", axis=0, tiled=True),
+        jnp.concatenate(
+            lax.all_to_all(jnp.stack([normed] * lax.axis_size("tp")), "tp", 0, 0), axis=0
+        ),
     )
     gate_val = jnp.einsum(
         "gerd,edf->gerf", arrived, expert_gate, preferred_element_type=jnp.float32

time: 282 us -> 269 us (0.954)
  waiting for transfers between devices: 164 us -> 122 us
  blocking collectives: 39.5 us -> 70.5 us
    all_to_all x0 -> x1, blocking collectives: none -> 31 us  [local(): lax.all_to_all(jnp.stack([normed] * lax.axis_size('tp')), 'tp', 0, 0)]
    reduce_scatter x1, waiting for transfers between devices: 44.9 us -> 23 us  [local(): lax.psum_scatter(partial_rows.astype(jnp.bfloat16), 'tp', scatter_dimensi...]
    all_gather x1 -> x0, waiting for transfers between devices: 20.4 us -> none  [local(): lax.all_gather(normed, 'tp', axis=0, tiled=True)]
  transfers between devices with their start and end apart: 7 -> 6, of which waited for: 5 -> 4; matrix products, arithmetic and copies ran while one was open for 12% -> 8% of each run, Pallas kernels for 0% -> 0%
where the time goes in v1:
time: 269 us
  waiting for transfers between devices  122 us (45%)
  blocking collectives  70.5 us (26%)
  local copies, waits for them, and re-layouts  20.9 us (8%)
  starting transfers between devices  15.1 us (6%)
  matrix products  14.5 us (5%)
  between operations  13.4 us (5%)
  other arithmetic  12.4 us (5%)
    all_gather x1, waiting for transfers between devices, local(): lax.all_gather(arrived, 'tp', axis=2, tiled=True)  46.1 us
    all_to_all x1, blocking collectives, local(): lax.all_to_all(outgoing, 'sp', split_axis=0, concat_axis=0, tiled=True)  39.5 us
    all_to_all x1, blocking collectives, local(): lax.all_to_all(jnp.stack([normed] * lax.axis_size('tp')), 'tp', 0, 0)  31 us
    all_to_all x1, waiting for transfers between devices, local(): lax.all_to_all(summed.astype(jnp.bfloat16), 'sp', split_axis=0, concat_ax...  26.7 us
    reduce_scatter x1, waiting for transfers between devices, local(): lax.psum_scatter(round_trip(jnp.dot(mixed_rows, out_weight, preferred_ele...  26.1 us
    reduce_scatter x1, waiting for transfers between devices, local(): lax.psum_scatter(partial_rows.astype(jnp.bfloat16), 'tp', scatter_dimensi...  23 us
    all_to_all x1, starting transfers between devices, local(): lax.all_to_all(summed.astype(jnp.bfloat16), 'sp', split_axis=0, concat_ax...  10.4 us
  transfers between devices with their start and end apart: 6, of which 4 were waited for; matrix products, arithmetic and copies ran while one was open for 8% of the time, Pallas kernels for 0%

profile of v1, /device:TPU:1, one launch (start us, length us, event | category | flops | bytes accessed | tf_op | source)
XLA Modules:
  0.0 268.8 jit_solution(6708056348959006757)
XLA Ops:
  6.5 0.0 copy-start
  6.5 0.0 reduce-scatter.4.cloned.1.call-start
  6.5 1.1 convert_multiply_fusion.2
  7.7 4.6 %collective-permute-start = (f32[2,256]{1,0:T(2,128)S(1)}, f32[2,256]{1,0:T(2,128)S(1)}, u32[]{:S(2)}, u32[]{:S(2)}) collective-permute-start(f32[2,256]{1,0:T(2,128)S(1)} %slice.40), channel_id=1, source_target_pairs={{0,4},{4,8},{8,12},{12,16},{16,20},{20,24},{24,28},{28,32},{32,36}... | collective-permute-start | bytes 6152 | tf_op jit(solution)/shard_map/ppermute | solution.py:10
  12.3 0.8 slice_convert_fusion.2
  13.1 0.0 collective-permute-done
  13.1 3.2 %convolution_convert_fusion.1 = bf16[384,2048]{1,0:T(8,128)(2,1)} fusion(bf16[256,2048]{1,0:T(8,128)(2,1)} %param.20, f32[2,256]{1,0:T(2,128)S(1)} %collective-permute-done, f32[384,256]{1,0:T(8,128)S(1)} %convert_multiply_fusion.2, bf16[384,256]{1,0:T(8,128)(2,1)} %param.16, f32[256]{0:T(256)S(1)} %bitcast.71, f32[256]{0:T(256)S(1)} %bitcast.72, ...), kind=kOutput, calls=%fused_computation.5 | convolution fusion | flops 404422656 | bytes 3216384 | tf_op jit(solution)/shard_map/dot_general | solution.py:64
  16.3 0.0 reduce-scatter.4.cloned.1.call-update
  16.3 0.0 copy-start.1
  16.3 0.0 all-gather.3.cloned.1.call-start
  16.4 0.6 copy-done.7
  16.9 0.1 copy.34
  17.1 0.2 reshape.98
  17.3 0.0 copy-start.6
  17.3 2.4 reduce-window.6
  19.7 0.1 slice.43
  19.9 0.1 copy.36
  20.0 0.1 reshape.135
  20.2 0.1 bitcast_bitcast_fusion
  20.3 0.1 fusion.26
  20.4 1.2 scatter_custom_fusion
  21.6 26.1 %reduce-scatter.4.cloned.1.call-done = bf16[96,2048]{1,0:T(8,128)(2,1)} async-done(((bf16[384,2048]{1,0:T(8,128)(2,1)}), bf16[96,2048]{1,0:T(8,128)(2,1)}) %reduce-scatter.4.cloned.1.call-update) | async-done | bytes 393232 | tf_op jit(solution)/shard_map/reduce_scatter | solution.py:63
  47.8 0.0 copy-done.1
  47.8 1.2 fusion.7
  49.0 0.0 copy-done.6
  49.0 1.2 fusion.9
  50.2 0.0 copy-start.3
  50.2 0.7 copy-done.3
  51.0 1.4 gather_fusion
  52.3 0.4 reshape.102
  52.8 39.5 %all_to_all.15 = bf16[64,4,2048]{2,1,0:T(4,128)(2,1)S(1)} all-to-all(bf16[64,4,2048]{2,1,0:T(4,128)(2,1)S(1)} %reshape.102), channel_id=1, replica_groups=mesh['sp'=64,'tp'=4] {'sp'}, dimensions={0} | all-to-all | bytes 2097152 | tf_op jit(solution)/shard_map/all_to_all | solution.py:85
  92.3 1.6 copy.39
  93.8 0.0 all-gather.3.cloned.1.call-update
  93.8 0.0 copy-start.10
  93.8 0.0 reduce-scatter.8.cloned.1.call-start
  93.9 46.1 %all-gather.3.cloned.1.call-done = bf16[64,16,2048]{2,0,1:T(8,128)(2,1)} async-done(((bf16[64,4,2048]{2,0,1:T(8,128)(2,1)}), bf16[64,16,2048]{2,0,1:T(8,128)(2,1)}) %all-gather.3.cloned.1.call-update) | async-done | bytes 4194320 | tf_op jit(solution)/shard_map/all_gather | solution.py:88
  140.0 0.0 copy-done.9
  140.0 3.6 %convolution_bitcast_fusion.1 = f32[64,1,16,256]{3,0,2,1:T(8,128)S(1)} fusion(bf16[64,16,2048]{2,0,1:T(8,128)(2,1)} %all-gather.3.cloned.1.call-done, bf16[1,2048,256]{2,1,0:T(8,128)(2,1)S(1)} %copy-done.9), kind=kOutput, calls=%fused_computation.9 | convolution fusion | flops 1073741824 | bytes 6291456 | tf_op jit(solution)/shard_map/gerd,edf->gerf/dot_general | solution.py:93
  143.6 0.0 copy-done.10
  143.6 0.0 copy-done.8
  143.6 1.3 fusion.2
  144.9 1.4 convert_bitcast_fusion
  146.3 4.2 %copy.41 = bf16[64,1,16,2048]{3,0,1,2:T(8,128)(2,1)} copy(bf16[64,1,16,2048]{3,2,0,1:T(8,128)(2,1)S(1)} %convert_bitcast_fusion) | data formatting | bytes 8388608 | tf_op jit(solution)/shard_map/optimization_barrier | solution.py:14
  150.5 0.0 reduce-scatter.8.cloned.1.call-update
  150.5 0.0 reduce-scatter.6.cloned.1.call-start
  150.6 0.9 copy-done.4
  151.5 0.2 stack.2
  151.7 0.0 copy-start.11
  151.7 31.0 %all_to_all.16 = bf16[4,96,2048]{2,1,0:T(8,128)(2,1)S(1)} all-to-all(bf16[4,96,2048]{2,1,0:T(8,128)(2,1)S(1)} %stack.2), channel_id=1, replica_groups=mesh['sp'=64,'tp'=4] {'tp'}, dimensions={0} | all-to-all | bytes 3145728 | tf_op jit(solution)/shard_map/all_to_all | solution.py:90
  182.7 0.6 fusion.38
  183.3 4.5 %convolution_convert_fusion = bf16[384,2048]{1,0:T(8,128)(2,1)} fusion(bf16[256,2048]{1,0:T(8,128)(2,1)} %param.29, bf16[384,2048]{1,0:T(8,128)(2,1)S(1)} %bitcast.69, bf16[2048,256]{1,0:T(8,128)(2,1)} %param.28, f32[384,256]{1,0:T(8,128)S(1)} %fusion.38), kind=kOutput, calls=%fused_computation.4 | convolution fusion | flops 806682624 | bytes 5636096 | tf_op jit(solution)/shard_map/dot_general | solution.py:105
  187.8 0.0 reduce-scatter.6.cloned.1.call-update
  187.8 23.0 %reduce-scatter.8.cloned.1.call-done = bf16[64,1,4,2048]{3,0,1,2:T(8,128)(2,1)} async-done(((bf16[64,1,16,2048]{3,0,1,2:T(8,128)(2,1)}), bf16[64,1,4,2048]{3,0,1,2:T(8,128)(2,1)}) %reduce-scatter.8.cloned.1.call-update) | async-done | bytes 1048592 | tf_op jit(solution)/shard_map/reduce_scatter | solution.py:108
  210.8 3.0 %copy.42 = bf16[64,1,4,2048]{3,2,1,0:T(4,128)(2,1)} copy(bf16[64,1,4,2048]{3,0,1,2:T(8,128)(2,1)} %reduce-scatter.8.cloned.1.call-done) | data formatting | bytes 2097152 | tf_op jit(solution)/shard_map/reduce_scatter | solution.py:108
  213.8 10.4 %all-to-all-start.2 = ((bf16[64,1,4,2048]{3,2,1,0:T(4,128)(2,1)}), bf16[64,1,4,2048]{3,2,1,0:T(4,128)(2,1)S(1)}, u32[]{:S(2)}, u32[]{:S(2)}) async-start(bf16[64,1,4,2048]{3,2,1,0:T(4,128)(2,1)} %copy.42), calls=%async_computation.5 | async-start | bytes 2097152 | tf_op jit(solution)/shard_map/all_to_all | solution.py:115
  224.3 0.8 constant_dynamic-slice_fusion
  225.0 0.7 copy.43
  225.7 26.7 %all-to-all-done.2 = bf16[64,1,4,2048]{3,2,1,0:T(4,128)(2,1)S(1)} async-done(((bf16[64,1,4,2048]{3,2,1,0:T(4,128)(2,1)}), bf16[64,1,4,2048]{3,2,1,0:T(4,128)(2,1)S(1)}, u32[]{:S(2)}, u32[]{:S(2)}) %all-to-all-start.2) | async-done | bytes 1048608 | tf_op jit(solution)/shard_map/all_to_all | solution.py:115
  252.4 0.3 reshape.109
  252.7 2.0 gather_fusion.1
  254.7 2.2 reshape.114
  256.9 3.2 %multiply_reduce_fusion = f32[96,2048]{1,0:T(8,128)} fusion(f32[96,2,2048]{2,1,0:T(2,128)S(1)} %reshape.114, f32[96,2]{1,0:T(8,128)S(1)} %copy-done.5), kind=kLoop, calls=%fused_computation.6 | loop fusion | flops 589824 | bytes 2360064 | tf_op jit(solution)/shard_map/reduce_sum | solution.py:121
  260.1 0.0 copy-done.2
  260.1 2.2 fusion.11
  (23 shorter events, 0.2 us)
Async XLA Ops:
  6.5 138.4 %copy-start = (bf16[1,256,2048]{2,1,0:T(8,128)(2,1)S(1)}, bf16[1,256,2048]{2,1,0:T(8,128)(2,1)}, u32[]{:S(2)}) copy-start(bf16[1,256,2048]{2,1,0:T(8,128)(2,1)} %param.26) | copy-start | bytes 3145732
  6.5 41.2 %reduce-scatter.4.cloned.1.call-start = ((), (), s32[]{:S(2)}) async-start(), calls=%async_computation.6 | async-start | bytes 1966080 | tf_op jit(solution)/shard_map/reduce_scatter | solution.py:63
  7.7 5.4 %collective-permute-start = (f32[2,256]{1,0:T(2,128)S(1)}, f32[2,256]{1,0:T(2,128)S(1)}, u32[]{:S(2)}, u32[]{:S(2)}) collective-permute-start(f32[2,256]{1,0:T(2,128)S(1)} %slice.40), channel_id=1, source_target_pairs={{0,4},{4,8},{8,12},{12,16},{16,20},{20,24},{24,28},{28,32},{32,36}... | collective-permute-start | bytes 6152 | tf_op jit(solution)/shard_map/ppermute | solution.py:10
  16.3 0.7 copy-start.7
  16.3 31.5 %copy-start.1 = (bf16[96,2048]{1,0:T(8,128)(2,1)S(1)}, bf16[96,2048]{1,0:T(8,128)(2,1)}, u32[]{:S(2)}) copy-start(bf16[96,2048]{1,0:T(8,128)(2,1)} %param.15) | copy-start | bytes 1179652
  16.3 123.7 %all-gather.3.cloned.1.call-start = ((), (), s32[]{:S(2)}) async-start(), calls=%async_computation.9 | async-start | bytes 5242880 | tf_op jit(solution)/shard_map/all_gather | solution.py:88
  17.3 31.7 %copy-start.6 = (f32[2048]{0:T(1024)S(1)}, f32[2048]{0:T(1024)}, u32[]{:S(2)}) copy-start(f32[2048]{0:T(1024)} %param.21) | copy-start | bytes 24580
  50.2 0.7 copy-start.3
  92.3 47.7 %copy-start.9 = (bf16[1,2048,256]{2,1,0:T(8,128)(2,1)S(1)}, bf16[1,2048,256]{2,1,0:T(8,128)(2,1)}, u32[]{:S(2)}) copy-start(bf16[1,2048,256]{2,1,0:T(8,128)(2,1)} %param.24) | copy-start | bytes 3145732
  93.8 49.7 %copy-start.10 = (bf16[1,2048,256]{2,1,0:T(8,128)(2,1)S(1)}, bf16[1,2048,256]{2,1,0:T(8,128)(2,1)}, u32[]{:S(2)}) copy-start(bf16[1,2048,256]{2,1,0:T(8,128)(2,1)} %param.25) | copy-start | bytes 3145732
  93.8 117.0 %reduce-scatter.8.cloned.1.call-start = ((), (), s32[]{:S(2)}) async-start(), calls=%async_computation.8 | async-start | bytes 5242880 | tf_op jit(solution)/shard_map/reduce_scatter | solution.py:108
  140.0 3.6 %copy-start.8 = (bf16[64,16,2048]{2,0,1:T(8,128)(2,1)S(1)}, bf16[64,16,2048]{2,0,1:T(8,128)(2,1)}, u32[]{:S(2)}) copy-start(bf16[64,16,2048]{2,0,1:T(8,128)(2,1)} %all-gather.3.cloned.1.call-done) | copy-start | bytes 12582916
  150.5 1.0 copy-start.4
  150.5 109.6 %reduce-scatter.6.cloned.1.call-start = ((), (), s32[]{:S(2)}) async-start(), calls=%async_computation.7 | async-start | bytes 1966080 | tf_op jit(solution)/shard_map/reduce_scatter | solution.py:111
  151.7 31.0 %copy-start.11 = (bf16[2048,256]{1,0:T(8,128)(2,1)S(1)}, bf16[2048,256]{1,0:T(8,128)(2,1)}, u32[]{:S(2)}) copy-start(bf16[2048,256]{1,0:T(8,128)(2,1)} %param.27) | copy-start | bytes 3145732
  213.8 38.6 %all-to-all-start.2 = ((bf16[64,1,4,2048]{3,2,1,0:T(4,128)(2,1)}), bf16[64,1,4,2048]{3,2,1,0:T(4,128)(2,1)S(1)}, u32[]{:S(2)}, u32[]{:S(2)}) async-start(bf16[64,1,4,2048]{3,2,1,0:T(4,128)(2,1)} %copy.42), calls=%async_computation.5 | async-start | bytes 2097152 | tf_op jit(solution)/shard_map/all_to_all | solution.py:115
  254.7 2.2 copy-start.5
  256.9 3.2 %copy-start.2 = (bf16[96,2048]{1,0:T(8,128)(2,1)S(1)}, bf16[96,2048]{1,0:T(8,128)(2,1)}, u32[]{:S(2)}) copy-start(bf16[96,2048]{1,0:T(8,128)(2,1)} %reduce-scatter.4.cloned.1.call-done) | copy-start | bytes 1179652
Sparse Core Ops, SparseCore 0:
  16.4 31.3 reduce-scatter.3
  94.0 45.9 all-gather.2
  150.7 60.0 reduce-scatter.7
  213.2 26.8 reduce-scatter.5
